TPU v7x, 32 devices: a whole 2x2x4 slice. The times are simulated.
32 devices in a mesh: sp: 8 (over z, y), tp: 4 (over x, core).
Axes of the slice: x: 2, y: 2, z: 4, core: 2. Of those that a mesh axis runs over, the one named last changes fastest.
Arguments:
- residual: bfloat16 [1024, 2048], P(('sp', 'tp')), may hold values from -6 to 6
- query_content: bfloat16 [1024, 1024], P('sp', 'tp'), may hold values from -400 to 400
- query_rotary: bfloat16 [1024, 384], P('sp', 'tp'), may hold values from -16 to 16
- key_latent: bfloat16 [1024, 512], P('sp'), may hold values from -6 to 6
- rotary_key: bfloat16 [1024, 32], P('sp'), may hold values from -6 to 6
- latent_gain: float32 [512], replicated, may hold values from 0.1 to 1.9
- key_weight: bfloat16 [512, 1024], P(None, 'tp'), may hold values from -0.25 to 0.25
- value_weight: bfloat16 [512, 1024], P(None, 'tp'), may hold values from -0.25 to 0.25
- output_gain: float32 [1024], P('tp'), may hold values from 0.1 to 1.9
- output_weight: bfloat16 [1024, 2048], P('tp'), may hold values from -0.1875 to 0.1875
- mixer_gain: float32 [2048], replicated, may hold values from 0.1 to 1.9
- gate_weight: bfloat16 [2048, 5632], P('sp', 'tp'), may hold values from -0.125 to 0.125
- up_weight: bfloat16 [2048, 5632], P('sp', 'tp'), may hold values from -0.125 to 0.125
- down_weight: bfloat16 [5632, 2048], P('tp', 'sp'), may hold values from -0.078125 to 0.078125
Outputs:
- layer_out: bfloat16 [1024, 2048], P(('sp', 'tp'))
All inputs are finite; a program needn't handle non-finite values.
Results may differ from a plain program's by a relative error of at most 0.015.
Values may be sent and summed in bfloat16 or wider, within the bound.
A program may use at most 128 MiB of HBM per device.

v0:
```python
import jax
import jax.numpy as jnp
from jax import lax
from jax.sharding import PartitionSpec as P

NARROW_HEADS = 8
WIDE_HEADS = 4
NARROW_DIM = 64
WIDE_DIM = 128
ROT_DIM = 32


epsilon = 1e-06
rope_base = 500000.0


def normalize(values):
    values = values.astype(jnp.float32)
    return values * lax.rsqrt(jnp.mean(values * values, axis=-1, keepdims=True) + epsilon)


def rotate(values, positions):
    half_width = values.shape[-1] // 2
    inverse = 1.0 / jnp.power(
        rope_base, jnp.arange(0, 2 * half_width, 2, dtype=jnp.float32) / (2 * half_width)
    )
    angles = positions.astype(jnp.float32)[:, None] * inverse[None, :]
    table_shape = (angles.shape[0],) + (1,) * (values.ndim - 2) + (half_width,)
    cosine_table = jnp.cos(angles).reshape(table_shape)
    sine_table = jnp.sin(angles).reshape(table_shape)
    first_half = values[..., :half_width]
    second_half = values[..., half_width:]
    return jnp.concatenate(
        [
            first_half * cosine_table - second_half * sine_table,
            second_half * cosine_table + first_half * sine_table,
        ],
        axis=-1,
    )


def group_update(carried, query_part, rotary_part, key_part, rotary_keys, value_part, factor):
    running_max, totals, accumulated = carried
    scores = (
        jnp.einsum("qhd,khd->hqk", query_part, key_part, preferred_element_type=jnp.float32)
        + jnp.einsum("qhd,kd->hqk", rotary_part, rotary_keys, preferred_element_type=jnp.float32)
    ) * factor
    new_max = jnp.max(scores, axis=-1)
    shrink = jnp.exp(running_max - new_max)
    powers = jnp.exp(scores - new_max[..., None])
    totals = totals * shrink + jnp.sum(powers, axis=-1)
    added = jnp.einsum(
        "hqk,khd->qhd", powers.astype(jnp.bfloat16), value_part, preferred_element_type=jnp.float32
    )
    accumulated = accumulated * jnp.transpose(shrink)[:, :, None] + added
    return (new_max, totals, accumulated)


def on_device(
    residual,
    query_content,
    query_rotary,
    key_latent,
    rotary_key,
    latent_gain,
    key_weight,
    value_weight,
    output_gain,
    output_weight,
    mixer_gain,
    gate_weight,
    up_weight,
    down_weight,
):
    tp_count = lax.axis_size("tp")
    narrow_dev = NARROW_HEADS // tp_count
    wide_dev = WIDE_HEADS // tp_count
    row_count = key_latent.shape[0]
    positions = lax.axis_index("sp") * row_count + lax.iota(jnp.int32, row_count)
    latent = (normalize(key_latent) * latent_gain).astype(jnp.bfloat16)
    key_rows = jnp.dot(latent, key_weight, preferred_element_type=jnp.float32).astype(jnp.bfloat16)
    value_rows = jnp.dot(latent, value_weight, preferred_element_type=jnp.float32).astype(
        jnp.bfloat16
    )
    rot_keys = rotate(rotary_key.astype(jnp.float32), positions).astype(jnp.bfloat16)
    head_count = narrow_dev + wide_dev
    rot_queries = rotate(
        query_rotary.astype(jnp.float32).reshape(row_count, head_count, ROT_DIM), positions
    ).astype(jnp.bfloat16)
    narrow_cols = narrow_dev * NARROW_DIM
    query_narrow = query_content[:, :narrow_cols].reshape(row_count, narrow_dev, NARROW_DIM)
    query_wide = query_content[:, narrow_cols:].reshape(row_count, wide_dev, WIDE_DIM)
    rotary_narrow = rot_queries[:, :narrow_dev]
    rotary_wide = rot_queries[:, narrow_dev:]
    narrow_factor = (NARROW_DIM + ROT_DIM) ** (-0.5)
    wide_factor = (WIDE_DIM + ROT_DIM) ** (-0.5)

    def start_state(count, width):
        return (
            jnp.full((count, row_count), -jnp.inf, jnp.float32),
            jnp.zeros((count, row_count), jnp.float32),
            jnp.zeros((row_count, count, width), jnp.float32),
        )

    carried = (start_state(narrow_dev, NARROW_DIM), start_state(wide_dev, WIDE_DIM))
    piece_keys = lax.all_gather(key_rows, "sp", axis=0, tiled=True)
    piece_rotary = lax.all_gather(rot_keys, "sp", axis=0, tiled=True)
    piece_values = lax.all_gather(value_rows, "sp", axis=0, tiled=True)
    length = piece_keys.shape[0]
    narrow_keys = piece_keys[:, :narrow_cols].reshape(length, narrow_dev, NARROW_DIM)
    wide_keys = piece_keys[:, narrow_cols:].reshape(length, wide_dev, WIDE_DIM)
    narrow_values = piece_values[:, :narrow_cols].reshape(length, narrow_dev, NARROW_DIM)
    wide_values = piece_values[:, narrow_cols:].reshape(length, wide_dev, WIDE_DIM)
    narrow_state = group_update(
        carried[0],
        query_narrow,
        rotary_narrow,
        narrow_keys,
        piece_rotary,
        narrow_values,
        narrow_factor,
    )
    wide_state = group_update(
        carried[1], query_wide, rotary_wide, wide_keys, piece_rotary, wide_values, wide_factor
    )
    narrow_state, wide_state = (narrow_state, wide_state)

    def finish(carried):
        return normalize(carried[2] / jnp.transpose(carried[1])[:, :, None]).reshape(row_count, -1)

    mixed = (
        jnp.concatenate([finish(narrow_state), finish(wide_state)], axis=1) * output_gain
    ).astype(jnp.bfloat16)
    whole_output = lax.all_gather(output_weight, "tp", axis=0, tiled=True)
    regrouped = lax.all_to_all(mixed, "tp", split_axis=0, concat_axis=1, tiled=True)
    projected = jnp.dot(regrouped, whole_output, preferred_element_type=jnp.float32)
    middle = (residual.astype(jnp.float32) + projected).astype(jnp.bfloat16)
    normed = (normalize(middle) * mixer_gain).astype(jnp.bfloat16)
    block_normed = lax.all_gather(normed, "tp", axis=0, tiled=True)
    gate_sums = jnp.dot(
        block_normed,
        lax.all_gather(gate_weight, "sp", axis=0, tiled=True),
        preferred_element_type=jnp.float32,
    )
    up_sums = jnp.dot(
        block_normed,
        lax.all_gather(up_weight, "sp", axis=0, tiled=True),
        preferred_element_type=jnp.float32,
    )
    down_whole = lax.all_gather(down_weight, "sp", axis=1, tiled=True)
    hidden = (jax.nn.silu(gate_sums) * up_sums).astype(jnp.bfloat16)
    channel_out = lax.psum_scatter(
        jnp.dot(hidden, down_whole, preferred_element_type=jnp.float32).astype(jnp.bfloat16),
        "tp",
        scatter_dimension=0,
        tiled=True,
    ).astype(jnp.float32)
    return (middle.astype(jnp.float32) + channel_out).astype(jnp.bfloat16)


def solution(mesh):
    placed = (
        P(("sp", "tp"), None),
        P("sp", "tp"),
        P("sp", "tp"),
        P("sp", None),
        P("sp", None),
        P(),
        P(None, "tp"),
        P(None, "tp"),
        P("tp"),
        P("tp", None),
        P(),
        P("sp", "tp"),
        P("sp", "tp"),
        P("tp", "sp"),
    )
    return jax.shard_map(
        on_device, mesh=mesh, in_specs=placed, out_specs=P(("sp", "tp"), None), check_vma=False
    )
```

profile of v0, /device:TPU:0, one launch (start us, length us, event | category | flops | bytes accessed | tf_op | source)
XLA Modules:
  0.0 365.0 jit_solution(12464630408035600343)
XLA Ops:
  6.5 0.7 all-gather.5.cloned.1.call-update
  7.3 0.7 all-gather.7.cloned.1.call-update
  8.1 0.7 all-gather.11.cloned.1.call-update
  8.8 0.5 all-gather.9.cloned.1.call-update
  9.4 0.7 convert_element_type.65
  10.1 0.7 convert.17
  10.8 1.0 fusion.18
  11.9 1.2 convolution_convert_fusion.2
  13.0 33.2 %all_gather.24 = bf16[1024,256]{1,0:T(8,128)(2,1)S(1)} all-gather(bf16[128,256]{1,0:T(8,128)(2,1)S(1)} %convolution_convert_fusion.2), channel_id=1, replica_groups=mesh['sp'=8,'tp'=4] {'sp'}, dimensions={0}, use_global_device_ids=true | all-gather | bytes 589824 | tf_op jit(solution)/shard_map/all_gather | solution.py:106
  46.2 0.1 copy.20
  46.4 0.8 slice.37
  47.3 1.3 convolution_convert_fusion.1
  48.6 33.4 %all_gather.26 = bf16[1024,256]{1,0:T(8,128)(2,1)S(1)} all-gather(bf16[128,256]{1,0:T(8,128)(2,1)S(1)} %convolution_convert_fusion.1), channel_id=1, replica_groups=mesh['sp'=8,'tp'=4] {'sp'}, dimensions={0}, use_global_device_ids=true | all-gather | bytes 589824 | tf_op jit(solution)/shard_map/all_gather | solution.py:108
  82.3 27.2 %all_gather.25 = bf16[1024,32]{0,1:T(8,128)(2,1)S(1)} all-gather(bf16[128,32]{0,1:T(8,128)(2,1)S(1)} %pad_maximum_fusion.1), channel_id=1, replica_groups=mesh['sp'=8,'tp'=4] {'sp'}, dimensions={0}, use_global_device_ids=true | all-gather | bytes 73728 | tf_op jit(solution)/shard_map/all_gather | solution.py:107
  109.5 0.3 convolution_bitcast_fusion.1
  109.9 0.4 fusion.41
  110.2 0.2 fusion.11
  110.4 0.3 multiply_reduce_fusion.2
  111.0 0.3 convolution_bitcast_fusion.2
  111.3 0.3 fusion.40
  111.6 0.2 fusion.15
  111.8 0.4 multiply_reduce_fusion.1
  112.3 6.5 %all_to_all.16 = bf16[4,32,256]{2,1,0:T(8,128)(2,1)S(1)} all-to-all(bf16[4,32,256]{2,1,0:T(8,128)(2,1)S(1)} %fusion.26), channel_id=1, replica_groups=mesh['sp'=8,'tp'=4] {'tp'}, dimensions={0} | all-to-all | bytes 131072 | tf_op jit(solution)/shard_map/all_to_all | solution.py:135
  118.8 3.1 multiply_reduce_fusion
  122.1 7.0 %all_gather.28 = bf16[128,2048]{1,0:T(8,128)(2,1)S(1)} all-gather(bf16[32,2048]{1,0:T(8,128)(2,1)S(1)} %multiply_convert_fusion), channel_id=1, replica_groups=mesh['sp'=8,'tp'=4] {'tp'}, dimensions={0}, use_global_device_ids=true | all-gather | bytes 655360 | tf_op jit(solution)/shard_map/all_gather | solution.py:139
  129.0 14.8 %all-gather.7.cloned.1.call-done = bf16[2048,1408]{1,0:T(8,128)(2,1)} async-done(((bf16[256,1408]{1,0:T(8,128)(2,1)}), bf16[2048,1408]{1,0:T(8,128)(2,1)}) %all-gather.7.cloned.1.call-update) | async-done | bytes 5767184 | tf_op jit(solution)/shard_map/all_gather | solution.py:142
  143.9 3.6 fusion.42
  147.5 89.8 %all-gather.11.cloned.1.call-done = bf16[1408,2048]{1,0:T(8,128)(2,1)} async-done(((bf16[1408,256]{1,0:T(8,128)(2,1)}), bf16[1408,2048]{1,0:T(8,128)(2,1)}) %all-gather.11.cloned.1.call-update) | async-done | bytes 5767184 | tf_op jit(solution)/shard_map/all_gather | solution.py:150
  237.3 92.6 %all-gather.9.cloned.1.call-done = bf16[2048,1408]{1,0:T(8,128)(2,1)} async-done(((bf16[256,1408]{1,0:T(8,128)(2,1)}), bf16[2048,1408]{1,0:T(8,128)(2,1)}) %all-gather.9.cloned.1.call-update) | async-done | bytes 5767184 | tf_op jit(solution)/shard_map/all_gather | solution.py:147
  329.9 7.0 %convolution_convert_fusion = bf16[128,2048]{1,0:T(8,128)(2,1)} fusion(bf16[1408,2048]{1,0:T(8,128)(2,1)} %all-gather.11.cloned.1.call-done, bf16[128,2048]{1,0:T(8,128)(2,1)S(1)} %all_gather.28, bf16[2048,1408]{1,0:T(8,128)(2,1)} %all-gather.9.cloned.1.call-done, f32[128,1408]{1,0:T(8,128)S(1)} %fusion.42), kind=kOutput, calls=%fused_computation.2 | convolution fusion | flops 1477738496 | bytes 13303808 | tf_op jit(solution)/shard_map/dot_general | solution.py:153
  336.9 20.0 %reduce-scatter.2.cloned.1.call-done = bf16[32,2048]{1,0:T(8,128)(2,1)} async-done(((bf16[128,2048]{1,0:T(8,128)(2,1)}), bf16[32,2048]{1,0:T(8,128)(2,1)}) %reduce-scatter.2.cloned.1.call-update) | async-done | bytes 131088 | tf_op jit(solution)/shard_map/reduce_scatter | solution.py:152
  356.9 1.6 add_convert_fusion
  (40 shorter events, 1.2 us)
Async XLA Ops:
  6.5 5.3 %copy-start = (bf16[512,256]{1,0:T(8,128)(2,1)S(1)}, bf16[512,256]{1,0:T(8,128)(2,1)}, u32[]{:S(2)}) copy-start(bf16[512,256]{1,0:T(8,128)(2,1)} %param.20) | copy-start | bytes 786436
  6.5 112.3 %all-gather.5.cloned.1.call-start = ((), (), s32[]{:S(2)}) async-start(), calls=%async_computation.2 | async-start | bytes 5242880 | tf_op jit(solution)/shard_map/all_gather | solution.py:134
  7.3 136.6 %all-gather.7.cloned.1.call-start = ((), (), s32[]{:S(2)}) async-start(), calls=%async_computation.3 | async-start | bytes 6488064 | tf_op jit(solution)/shard_map/all_gather | solution.py:142
  8.0 229.3 %all-gather.11.cloned.1.call-start = ((), (), s32[]{:S(2)}) async-start(), calls=%async_computation.5 | async-start | bytes 6488064 | tf_op jit(solution)/shard_map/all_gather | solution.py:150
  8.7 321.1 %all-gather.9.cloned.1.call-start = ((), (), s32[]{:S(2)}) async-start(), calls=%async_computation.4 | async-start | bytes 6488064 | tf_op jit(solution)/shard_map/all_gather | solution.py:147
  9.3 347.6 %reduce-scatter.2.cloned.1.call-start = ((), (), s32[]{:S(2)}) async-start(), calls=%async_computation.6 | async-start | bytes 655360 | tf_op jit(solution)/shard_map/reduce_scatter | solution.py:152
  11.8 99.4 %copy-start.2 = (bf16[128,256]{1,0:T(8,128)(2,1)S(1)}, bf16[128,256]{1,0:T(8,128)(2,1)}, u32[]{:S(2)}) copy-start(bf16[128,256]{1,0:T(8,128)(2,1)} %param.15) | copy-start | bytes 196612
  82.0 30.3 %copy-start.4 = (f32[256]{0:T(256)S(1)}, f32[256]{0:T(256)}, u32[]{:S(2)}) copy-start(f32[256]{0:T(256)} %param.22) | copy-start | bytes 3076
  82.0 36.8 %copy-start.1 = (bf16[32,2048]{1,0:T(8,128)(2,1)S(1)}, bf16[32,2048]{1,0:T(8,128)(2,1)}, u32[]{:S(2)}) copy-start(bf16[32,2048]{1,0:T(8,128)(2,1)} %param.14) | copy-start | bytes 393220
  110.2 11.7 %copy-start.3 = (f32[2048]{0:T(1024)S(1)}, f32[2048]{0:T(1024)}, u32[]{:S(2)}) copy-start(f32[2048]{0:T(1024)} %param.24) | copy-start | bytes 24580
Sparse Core Ops, SparseCore 0:
  8.9 37.1 all-gather.4
  48.3 95.5 all-gather.6
  145.9 91.3 all-gather.10
  239.3 90.4 all-gather.8
  337.0 19.8 reduce-scatter.1
where the time goes:
time: 366 us; the launch traced here: 365 us
  waiting for transfers between devices  220 us (60%)
  blocking collectives  107 us (29%)
  matrix products  18.2 us (5%)
  between operations  13.4 us (4%)
  other arithmetic  4.79 us (1%)
    all_gather x1, waiting for transfers between devices, on_device(): lax.all_gather(up_weight, 'sp', axis=0, tiled=True)  92.6 us
    all_gather x1, waiting for transfers between devices, on_device(): down_whole = lax.all_gather(down_weight, 'sp', axis=1, tiled=True)  89.8 us
    all_gather x1, blocking collectives, on_device(): piece_values = lax.all_gather(value_rows, 'sp', axis=0, tiled=True)  33.4 us
    all_gather x1, blocking collectives, on_device(): piece_keys = lax.all_gather(key_rows, 'sp', axis=0, tiled=True)  33.2 us
    all_gather x1, blocking collectives, on_device(): piece_rotary = lax.all_gather(rot_keys, 'sp', axis=0, tiled=True)  27.2 us
    reduce_scatter x1, waiting for transfers between devices, on_device(): lax.psum_scatter(jnp.dot(hidden, down_whole, preferred_element_type=jnp.f...  20 us
    all_gather x1, waiting for transfers between devices, on_device(): lax.all_gather(gate_weight, 'sp', axis=0, tiled=True)  14.8 us
  transfers between devices with their start and end apart: 5, of which 4 were waited for; matrix products, arithmetic and copies ran while one was open for 4% of the time, Pallas kernels for 0%

commit v1 on v0

--- a/solution.py
+++ b/solution.py
@@ -1,6 +1,11 @@
+import functools
+
 import jax
 import jax.numpy as jnp
+import numpy as np
 from jax import lax
+from jax.experimental import pallas as pl
+from jax.experimental.pallas import tpu as pltpu
 from jax.sharding import PartitionSpec as P
 
 NARROW_HEADS = 8
@@ -158,7 +163,454 @@
     return (middle.astype(jnp.float32) + channel_out).astype(jnp.bfloat16)
 
 
+MESH = pl.DeviceIdType.MESH
+LANES = 128
+PAIR = 2
+CHUNKS = 4
+
+
+def kernel(
+    n_sp,
+    query_ref,
+    turn_ref,
+    latent_ref,
+    rotary_ref,
+    latent_gain_ref,
+    key_weight_ref,
+    value_weight_ref,
+    output_gain_ref,
+    mixer_gain_ref,
+    cos_ref,
+    sin_ref,
+    swap_ref,
+    residual_ref,
+    output_weight_ref,
+    gate_ref,
+    up_ref,
+    down_ref,
+    out_ref,
+    lat_all,
+    rot_all,
+    keys,
+    values,
+    res_all,
+    out_all,
+    mix_all,
+    middle,
+    normed,
+    gate_all,
+    up_all,
+    down_all,
+    hidden,
+    part,
+    from_core,
+    to_x,
+    from_x,
+    to_z,
+    from_z,
+    send_sems,
+    recv_sems,
+    local_sems,
+):
+    n_z = n_sp // PAIR
+    s = lax.axis_index("sp")
+    t = lax.axis_index("tp")
+    z, y = s // PAIR, lax.rem(s, PAIR)
+    x, c = t // PAIR, lax.rem(t, PAIR)
+    rows, depth = latent_ref.shape
+    half = rows // PAIR
+    sibling = (s, x * PAIR + 1 - c)
+    across = (s, (1 - x) * PAIR + c)
+    beside = (z * PAIR + 1 - y, t)
+    f32 = jnp.float32
+
+    def z_id(step):
+        return (lax.rem(z + step, n_z) * PAIR + y, t)
+
+    barrier = pltpu.get_barrier_semaphore()
+    greeted = [(lax.rem(s + k, n_sp), t) for k in range(1, n_sp)] + [sibling, across]
+    for device in greeted:
+        pl.semaphore_signal(barrier, inc=1, device_id=device, device_id_type=MESH)
+
+    used = [0]
+    locals_used = [0]
+    sent = []
+
+    def local(src, dst):
+        copy = pltpu.make_async_copy(src, dst, local_sems.at[locals_used[0]])
+        locals_used[0] += 1
+        copy.start()
+        return copy
+
+    def send(src, dst, device):
+        copy = pltpu.make_async_remote_copy(
+            src_ref=src,
+            dst_ref=dst,
+            send_sem=send_sems.at[used[0]],
+            recv_sem=recv_sems.at[used[0]],
+            device_id=device,
+            device_id_type=MESH,
+        )
+        used[0] += 1
+        copy.start()
+        sent.append(copy)
+        return copy
+
+    width = gate_all.shape[1]
+    total_width = gate_ref.shape[1]
+    slab = gate_ref.shape[0]
+
+    def first(piece):
+        return pl.multiple_of(jnp.minimum(piece * width, total_width - width), LANES)
+
+    def span(owner):
+        return pl.ds(pl.multiple_of(owner * slab, slab), slab)
+
+    mine = span(s)
+    my_piece = pl.ds(first(z), width)
+    half_rows = pl.ds(pl.multiple_of(c * half, half), half)
+    locals_first = [
+        local(latent_ref, lat_all.at[pl.ds(pl.multiple_of(s * rows, rows), rows)]),
+        local(rotary_ref, rot_all.at[pl.ds(pl.multiple_of(s * rows, rows), rows)]),
+    ]
+    locals_rest = [
+        local(residual_ref, res_all.at[x, c, z]),
+        local(output_weight_ref, out_all.at[x, c]),
+        local(gate_ref.at[:, my_piece], gate_all.at[mine]),
+        local(up_ref.at[:, my_piece], up_all.at[mine]),
+        local(down_ref.at[my_piece], down_all.at[:, mine]),
+    ]
+    pl.semaphore_wait(barrier, len(greeted))
+
+    def token_half(owner):
+        return pl.ds(pl.multiple_of(owner * rows + c * half, half), half)
+
+    def send_latent(step):
+        device = (lax.rem(s + step, n_sp), t)
+        return (
+            send(latent_ref.at[half_rows], lat_all.at[token_half(s)], device),
+            send(rotary_ref.at[half_rows], rot_all.at[token_half(s)], device),
+        )
+
+    latent_copies = [send_latent(k) for k in range(1, n_sp)]
+    weight_x = send(output_weight_ref, out_all.at[x, c], across)
+    residual_z = [send(residual_ref, res_all.at[x, c, z], z_id(k)) for k in range(1, n_z)]
+    weight_y = [
+        send(gate_ref.at[:, my_piece], gate_all.at[mine], beside),
+        send(up_ref.at[:, my_piece], up_all.at[mine], beside),
+        send(down_ref.at[my_piece], down_all.at[:, mine], beside),
+    ]
+
+    latent_core = []
+    for step in range(1, n_sp):
+        for copy in latent_copies[step - 1]:
+            copy.wait_recv()
+        place = token_half(lax.rem(s + n_sp - step, n_sp))
+        latent_core.append(send(lat_all.at[place], lat_all.at[place], sibling))
+        latent_core.append(send(rot_all.at[place], rot_all.at[place], sibling))
+    weight_core = send(output_weight_ref, out_all.at[x, c], sibling)
+    for copy in locals_first:
+        copy.wait()
+    for copy in latent_core:
+        copy.wait_recv()
+
+    gain = latent_gain_ref[...]
+
+    def project(block, _):
+        place = pl.ds(pl.multiple_of(block * rows, rows), rows)
+        raw = lat_all[place, :].astype(f32)
+        scale = lax.rsqrt(jnp.mean(raw * raw, axis=-1, keepdims=True) + epsilon)
+        latent = (raw * scale * gain).astype(jnp.bfloat16)
+        keys[place, :] = jnp.dot(latent, key_weight_ref[...], preferred_element_type=f32).astype(
+            jnp.bfloat16
+        )
+        values[place, :] = jnp.dot(
+            latent, value_weight_ref[...], preferred_element_type=f32
+        ).astype(jnp.bfloat16)
+        return 0
+
+    lax.fori_loop(0, n_sp, project, 0)
+    rot_width = rot_all.shape[1]
+    rot_raw = rot_all[...]
+    swap = swap_ref[...]
+    rot_swapped = jnp.dot(rot_raw, swap[:rot_width, :rot_width], preferred_element_type=f32)
+    rot_keys = (
+        rot_raw.astype(f32) * cos_ref[:, :rot_width] + rot_swapped * sin_ref[:, :rot_width]
+    ).astype(jnp.bfloat16)
+    here = pl.ds(pl.multiple_of(s * rows, rows), rows)
+    turn_raw = turn_ref[...]
+    turn_swapped = jnp.dot(turn_raw, swap, preferred_element_type=f32)
+    turned = (turn_raw.astype(f32) * cos_ref[here, :] + turn_swapped * sin_ref[here, :]).astype(
+        jnp.bfloat16
+    )
+
+    content = query_ref.shape[1]
+    head_count = turn_ref.shape[1] // rot_width
+    wide_dev = (content - head_count * NARROW_DIM) // (WIDE_DIM - NARROW_DIM)
+    sizes = [NARROW_DIM] * (head_count - wide_dev) + [WIDE_DIM] * wide_dev
+    contract = (((1,), (1,)), ((), ()))
+    heads = []
+    start = 0
+    for index, size in enumerate(sizes):
+        cols = slice(start, start + size)
+        scores = lax.dot_general(
+            query_ref[:, cols], keys[:, cols], contract, preferred_element_type=f32
+        )
+        scores = scores + lax.dot_general(
+            turned[:, index * rot_width : (index + 1) * rot_width],
+            rot_keys,
+            contract,
+            preferred_element_type=f32,
+        )
+        scores = scores * (size + ROT_DIM) ** (-0.5)
+        powers = jnp.exp(scores - jnp.max(scores, axis=-1, keepdims=True))
+        totals = jnp.sum(powers, axis=-1, keepdims=True)
+        summed = jnp.dot(
+            powers.astype(jnp.bfloat16), values[:, cols], preferred_element_type=f32
+        )
+        attended = summed / totals
+        scale = lax.rsqrt(jnp.mean(attended * attended, axis=-1, keepdims=True) + epsilon)
+        heads.append(attended * scale)
+        start += size
+    mixed = (jnp.concatenate(heads, axis=1) * output_gain_ref[...]).astype(jnp.bfloat16)
+    mix_all[x, c, z] = mixed
+
+    mix_z = [send(mix_all.at[x, c, z], mix_all.at[x, c, z], z_id(k)) for k in range(1, n_z)]
+
+    def piece_of(step):
+        return pl.ds(first(lax.rem(z + step, n_z)), width)
+
+    gate_z = [
+        send(gate_ref.at[:, piece_of(k)], gate_all.at[mine], z_id(k)) for k in range(1, n_z)
+    ]
+    up_z = [send(up_ref.at[:, piece_of(k)], up_all.at[mine], z_id(k)) for k in range(1, n_z)]
+    down_z = [
+        send(down_ref.at[piece_of(k)], down_all.at[:, mine], z_id(k)) for k in range(1, n_z)
+    ]
+
+    for copy in residual_z:
+        copy.wait_recv()
+    for copy in locals_rest:
+        copy.wait()
+    residual_x = send(res_all.at[x, c], res_all.at[x, c], across)
+    for copy in mix_z:
+        copy.wait_recv()
+    mix_x = send(mix_all.at[x, c], mix_all.at[x, c], across)
+    mix_core = send(mix_all.at[x, c], mix_all.at[x, c], sibling)
+    residual_core = send(res_all.at[x, c], res_all.at[x, c], sibling)
+    weight_x.wait_recv()
+    weight_far = send(out_all.at[1 - x, c], out_all.at[1 - x, c], sibling)
+    mix_x.wait_recv()
+    mix_far = send(mix_all.at[1 - x, c], mix_all.at[1 - x, c], sibling)
+    residual_x.wait_recv()
+    residual_far = send(res_all.at[1 - x, c], res_all.at[1 - x, c], sibling)
+
+    def relay(copies, buffer, columns):
+        passed = []
+        for step in range(1, n_z):
+            copies[step - 1].wait_recv()
+            place = span(lax.rem(z + n_z - step, n_z) * PAIR + y)
+            block = buffer.at[:, place] if columns else buffer.at[place]
+            passed.append(send(block, block, beside))
+        return passed
+
+    for copy in (weight_core, weight_far, mix_core, mix_far, residual_core, residual_far):
+        copy.wait_recv()
+
+    mixer_gain = mixer_gain_ref[...]
+    d_model = middle.shape[1]
+
+    def finish_rows(block, _):
+        place = pl.ds(pl.multiple_of(block * rows, rows), rows)
+        total = res_all[:, :, block].reshape(rows, d_model).astype(f32)
+        projected = jnp.zeros((rows, d_model), f32)
+        for far in range(PAIR):
+            for core in range(PAIR):
+                projected = projected + jnp.dot(
+                    mix_all[far, core, block], out_all[far, core], preferred_element_type=f32
+                )
+        mid = (total + projected).astype(jnp.bfloat16)
+        middle[place, :] = mid
+        wide = mid.astype(f32)
+        scale = lax.rsqrt(jnp.mean(wide * wide, axis=-1, keepdims=True) + epsilon)
+        normed[place, :] = (wide * scale * mixer_gain).astype(jnp.bfloat16)
+        return 0
+
+    lax.fori_loop(0, n_z, finish_rows, 0)
+
+    gate_y = relay(gate_z, gate_all, False)
+    up_y = relay(up_z, up_all, False)
+    down_y = relay(down_z, down_all, True)
+    for copy in gate_y + up_y + weight_y[:2]:
+        copy.wait_recv()
+
+    lane = lax.broadcasted_iota(jnp.int32, (rows, width), 1)
+    fresh = lane + first(z) >= z * width
+
+    def units(block, _):
+        place = pl.ds(pl.multiple_of(block * rows, rows), rows)
+        left = normed[place, :]
+        gates = jnp.dot(left, gate_all[...], preferred_element_type=f32)
+        ups = jnp.dot(left, up_all[...], preferred_element_type=f32)
+        value = gates / (1.0 + jnp.exp(-gates)) * ups
+        hidden[place, :] = jnp.where(fresh, value, 0.0).astype(jnp.bfloat16)
+        return 0
+
+    lax.fori_loop(0, n_z, units, 0)
+    for copy in down_y + weight_y[2:]:
+        copy.wait_recv()
+
+    chunk = part.shape[-1]
+    core_copies = []
+    for n in range(CHUNKS):
+        product = jnp.dot(
+            hidden[...], down_all[:, n * chunk : (n + 1) * chunk], preferred_element_type=f32
+        )
+        part[n] = product.astype(jnp.bfloat16).reshape(part.shape[1:])
+        core_copies.append(send(part.at[n, :, :, 1 - c], from_core.at[n], sibling))
+    x_copies = []
+    for n in range(CHUNKS):
+        core_copies[n].wait_recv()
+        to_x[n] = (part[n, :, :, c].astype(f32) + from_core[n].astype(f32)).astype(jnp.bfloat16)
+        x_copies.append(send(to_x.at[n, :, 1 - x], from_x.at[n], across))
+    z_copies = []
+    for n in range(CHUNKS):
+        x_copies[n].wait_recv()
+        to_z[n] = (to_x[n, :, x].astype(f32) + from_x[n].astype(f32)).astype(jnp.bfloat16)
+        z_copies.append(
+            [
+                send(to_z.at[n, lax.rem(z + k, n_z)], from_z.at[n, k - 1], z_id(k))
+                for k in range(1, n_z)
+            ]
+        )
+    strip = out_ref.shape[0]
+    own = pl.ds(pl.multiple_of(z * rows + t * strip, strip), strip)
+    for n in range(CHUNKS):
+        total = to_z[n, z].astype(f32)
+        for k in range(1, n_z):
+            z_copies[n][k - 1].wait_recv()
+            total = total + from_z[n, k - 1].astype(f32)
+        cols = slice(n * chunk, (n + 1) * chunk)
+        out_ref[:, cols] = (middle[own, cols].astype(f32) + total).astype(jnp.bfloat16)
+    for copy in sent:
+        copy.wait_send()
+
+
+def fused(
+    n_sp,
+    residual,
+    query_content,
+    query_rotary,
+    key_latent,
+    rotary_key,
+    latent_gain,
+    key_weight,
+    value_weight,
+    output_gain,
+    output_weight,
+    mixer_gain,
+    gate_weight,
+    up_weight,
+    down_weight,
+):
+    n_z = n_sp // PAIR
+    rows, latent_width = key_latent.shape
+    strip, d_model = residual.shape
+    tokens = rows * n_sp
+    content = query_content.shape[1]
+    turn_width = query_rotary.shape[1]
+    half_width = ROT_DIM // 2
+    inverse = np.float32(1.0) / np.power(
+        np.float32(rope_base), np.arange(0, ROT_DIM, 2, dtype=np.float32) / np.float32(ROT_DIM)
+    )
+    angles = np.arange(tokens, dtype=np.float32)[:, None] * inverse[None, :].astype(np.float32)
+    head_count = turn_width // ROT_DIM
+    cosine = np.cos(angles).astype(np.float32)
+    sine = np.sin(angles).astype(np.float32)
+    cos_table = np.tile(np.concatenate([cosine, cosine], axis=1), (1, head_count))
+    sin_table = np.tile(np.concatenate([-sine, sine], axis=1), (1, head_count))
+    lane = np.arange(turn_width)
+    other = lane // ROT_DIM * ROT_DIM + (lane + half_width) % ROT_DIM
+    swap = np.zeros((turn_width, turn_width), np.float32)
+    swap[other, lane] = 1.0
+    tiles = gate_weight.shape[1] // LANES
+    width = -(-tiles // n_z) * LANES
+    slab = rows * n_z
+    chunk = d_model // CHUNKS
+    bf16 = jnp.bfloat16
+    n_copies = 2 * 2 * (n_sp - 1) + 8 * (n_z - 1) + 16 + CHUNKS * (n_z + 1)
+    vmem = pl.BlockSpec(memory_space=pltpu.VMEM)
+    anywhere = pl.BlockSpec(memory_space=pl.ANY)
+    return pl.pallas_call(
+        functools.partial(kernel, n_sp),
+        out_shape=jax.ShapeDtypeStruct((strip, d_model), bf16),
+        in_specs=[vmem] * 12 + [anywhere] * 5,
+        out_specs=vmem,
+        scratch_shapes=[
+            pltpu.VMEM((tokens, latent_width), bf16),
+            pltpu.VMEM((tokens, ROT_DIM), bf16),
+            pltpu.VMEM((tokens, content), bf16),
+            pltpu.VMEM((tokens, content), bf16),
+            pltpu.VMEM((PAIR, PAIR, n_z, strip, d_model), bf16),
+            pltpu.VMEM((PAIR, PAIR, content, d_model), bf16),
+            pltpu.VMEM((PAIR, PAIR, n_z, rows, content), bf16),
+            pltpu.VMEM((slab, d_model), bf16),
+            pltpu.VMEM((slab, d_model), bf16),
+            pltpu.VMEM((d_model, width), bf16),
+            pltpu.VMEM((d_model, width), bf16),
+            pltpu.VMEM((width, d_model), bf16),
+            pltpu.VMEM((slab, width), bf16),
+            pltpu.VMEM((CHUNKS, n_z, PAIR, PAIR, strip, chunk), bf16),
+            pltpu.VMEM((CHUNKS, n_z, PAIR, strip, chunk), bf16),
+            pltpu.VMEM((CHUNKS, n_z, PAIR, strip, chunk), bf16),
+            pltpu.VMEM((CHUNKS, n_z, strip, chunk), bf16),
+            pltpu.VMEM((CHUNKS, n_z, strip, chunk), bf16),
+            pltpu.VMEM((CHUNKS, n_z - 1, strip, chunk), bf16),
+            pltpu.SemaphoreType.DMA((n_copies,)),
+            pltpu.SemaphoreType.DMA((n_copies,)),
+            pltpu.SemaphoreType.DMA((8,)),
+        ],
+        compiler_params=pltpu.CompilerParams(
+            collective_id=0, has_side_effects=True, vmem_limit_bytes=60 * 1024 * 1024
+        ),
+        name="layer",
+    )(
+        query_content,
+        query_rotary,
+        key_latent,
+        rotary_key,
+        latent_gain.reshape(1, -1),
+        key_weight,
+        value_weight,
+        output_gain.reshape(1, -1),
+        mixer_gain.reshape(1, -1),
+        jnp.asarray(cos_table),
+        jnp.asarray(sin_table),
+        jnp.asarray(swap, dtype=bf16),
+        residual,
+        output_weight,
+        gate_weight,
+        up_weight,
+        down_weight,
+    )
+
+
 def solution(mesh):
+    n_sp, n_tp = mesh.shape["sp"], mesh.shape["tp"]
+
+    def program(*arrays):
+        residual, gate_weight = arrays[0], arrays[11]
+        fits = (
+            n_tp == PAIR * PAIR
+            and n_sp % PAIR == 0
+            and gate_weight.shape[0] % LANES == 0
+            and gate_weight.shape[1] % LANES == 0
+            and residual.shape[1] % (CHUNKS * LANES) == 0
+        )
+        if fits:
+            return fused(n_sp, *arrays)
+        return on_device(*arrays)
+
     placed = (
         P(("sp", "tp"), None),
         P("sp", "tp"),
@@ -176,5 +628,5 @@
         P("tp", "sp"),
     )
     return jax.shard_map(
-        on_device, mesh=mesh, in_specs=placed, out_specs=P(("sp", "tp"), None), check_vma=False
-    )
+        program, mesh=mesh, in_specs=placed, out_specs=P(("sp", "tp"), None), check_vma=False
+    )

time: 366 us -> 134 us (0.37)
  waiting for transfers between devices: 220 us -> 0 us
  Pallas kernels: 0 us -> 130 us
  blocking collectives: 107 us -> 0 us
  matrix products: 18.2 us -> 0 us
  between operations: 13.4 us -> 0.01 us
  other arithmetic: 4.79 us -> 0 us
    all_gather x4 -> x0, waiting for transfers between devices: 197 us -> none  [the longest x1 92.6 us: on_device(): lax.all_gather(up_weight, 'sp', axis=0, tiled=True)]
    pallas_call x0 -> x1, Pallas kernels: none -> 130 us  [fused(): pl.pallas_call(functools.partial(kernel, n_sp), out_shape=jax.ShapeDtypeS...]
    all_gather x4 -> x0, blocking collectives: 101 us -> none  [the longest x1 33.4 us: on_device(): piece_values = lax.all_gather(value_rows, 'sp', axis=0, tiled=True)]
    reduce_scatter x1 -> x0, waiting for transfers between devices: 20 us -> none  [on_device(): lax.psum_scatter(jnp.dot(hidden, down_whole, preferred_element_type=jnp.f...]
    dot_general x11 -> x0, matrix products: 18.2 us -> none  [the longest x1 7.03 us: on_device(): jnp.dot(hidden, down_whole, preferred_element_type=jnp.float32)]
    all_to_all x1 -> x0, blocking collectives: 6.49 us -> none  [on_device(): lax.all_to_all(mixed, 'tp', split_axis=0, concat_axis=1, tiled=True)]
    unnamed x10 -> x5, local copies, waits for them, and re-layouts: 0.03 us -> 3.75 us
  transfers between devices with their start and end apart: 5 -> 0, of which waited for: 4 -> 0; matrix products, arithmetic and copies ran while one was open for 4% -> 0% of each run, Pallas kernels for 0% -> 0%
where the time goes in v1:
time: 134 us
  Pallas kernels  130 us (97%)
  local copies, waits for them, and re-layouts  3.75 us (3%)
    pallas_call x1, Pallas kernels, fused(): pl.pallas_call(functools.partial(kernel, n_sp), out_shape=jax.ShapeDtypeS...  130 us
    unnamed x5, local copies, waits for them, and re-layouts  3.75 us

profile of v1, /device:TPU:0, one launch (start us, length us, event | category | flops | bytes accessed | tf_op | source)
XLA Modules:
  0.0 134.0 jit_solution(10188508978670630466)
XLA Ops:
  0.0 0.0 copy-start
  0.0 1.5 %copy.18.turn_ref = bf16[128,96]{1,0:T(8,128)(2,1)} copy(bf16[128,96]{0,1:T(8,128)(2,1)} %param.19) | data formatting | bytes 49152 | tf_op args[2]
  1.5 0.0 copy-done
  1.5 0.7 copy.19.rotary_ref
  2.2 130.3 %layer.1 = bf16[32,2048]{1,0:T(8,128)(2,1)} custom-call(bf16[128,256]{1,0:T(8,128)(2,1)} %query_ref.1, bf16[128,96]{1,0:T(8,128)(2,1)} %copy.18.turn_ref, bf16[128,512]{1,0:T(8,128)(2,1)} %latent_ref.1, bf16[128,32]{1,0:T(8,128)(2,1)} %copy.19.rotary_ref, f32[1,512]{1,0:T(1,128)} %bitcast.4, bf16[512,256]{1,0:T(8,128)(2,1)} %key_weight_ref.1, ...), custom_call_target="tpu_custom_call" | custom-call | tf_op jit(solution)/shard_map/layer/pallas_call | solution.py:544
  132.4 1.6 %copy.21 = bf16[32,2048]{1,0:T(8,128)(2,1)} copy(bf16[32,2048]{1,0:T(8,128)(2,1)} %layer.1) | data formatting | bytes 262144
Async XLA Ops:
  0.0 1.5 %copy-start = (bf16[128,32]{0,1:T(8,128)(2,1)S(1)}, bf16[128,32]{0,1:T(8,128)(2,1)}, u32[]{:S(2)}) copy-start(bf16[128,32]{0,1:T(8,128)(2,1)} %param.21) | copy-start | bytes 24580

commit v2 on v1

--- a/solution.py
+++ b/solution.py
@@ -166,15 +166,12 @@
 MESH = pl.DeviceIdType.MESH
 LANES = 128
 PAIR = 2
-CHUNKS = 4
 
 
 def kernel(
     n_sp,
     query_ref,
-    turn_ref,
     latent_ref,
-    rotary_ref,
     latent_gain_ref,
     key_weight_ref,
     value_weight_ref,
@@ -188,7 +185,10 @@
     gate_ref,
     up_ref,
     down_ref,
+    turn_hbm,
+    rotary_ref,
     out_ref,
+    turn_ref,
     lat_all,
     rot_all,
     keys,
@@ -208,6 +208,7 @@
     from_x,
     to_z,
     from_z,
+    summed_up,
     send_sems,
     recv_sems,
     local_sems,
@@ -269,45 +270,69 @@
     mine = span(s)
     my_piece = pl.ds(first(z), width)
     half_rows = pl.ds(pl.multiple_of(c * half, half), half)
+    here = pl.ds(pl.multiple_of(s * rows, rows), rows)
     locals_first = [
-        local(latent_ref, lat_all.at[pl.ds(pl.multiple_of(s * rows, rows), rows)]),
-        local(rotary_ref, rot_all.at[pl.ds(pl.multiple_of(s * rows, rows), rows)]),
+        local(latent_ref, lat_all.at[here]),
+        local(rotary_ref, rot_all.at[here]),
+        local(turn_hbm, turn_ref),
     ]
+    down_cols = pl.ds(pl.multiple_of(y * slab, slab), slab)
     locals_rest = [
         local(residual_ref, res_all.at[x, c, z]),
         local(output_weight_ref, out_all.at[x, c]),
         local(gate_ref.at[:, my_piece], gate_all.at[mine]),
         local(up_ref.at[:, my_piece], up_all.at[mine]),
-        local(down_ref.at[my_piece], down_all.at[:, mine]),
+        local(down_ref.at[my_piece], down_all.at[0, :, down_cols]),
     ]
     pl.semaphore_wait(barrier, len(greeted))
 
     def token_half(owner):
         return pl.ds(pl.multiple_of(owner * rows + c * half, half), half)
 
-    def send_latent(step):
-        device = (lax.rem(s + step, n_sp), t)
+    def send_latent(device):
         return (
             send(latent_ref.at[half_rows], lat_all.at[token_half(s)], device),
             send(rotary_ref.at[half_rows], rot_all.at[token_half(s)], device),
         )
 
-    latent_copies = [send_latent(k) for k in range(1, n_sp)]
+    def pass_latent(owner, device):
+        place = token_half(owner)
+        return (
+            send(lat_all.at[place], lat_all.at[place], device),
+            send(rot_all.at[place], rot_all.at[place], device),
+        )
+
+    def piece_of(step):
+        return pl.ds(first(lax.rem(z + step, n_z)), width)
+
+    latent_z = [send_latent(z_id(k)) for k in range(1, n_z)]
+    latent_y = [send_latent(beside)]
     weight_x = send(output_weight_ref, out_all.at[x, c], across)
-    residual_z = [send(residual_ref, res_all.at[x, c, z], z_id(k)) for k in range(1, n_z)]
+    gate_z = [
+        send(gate_ref.at[:, piece_of(k)], gate_all.at[mine], z_id(k)) for k in range(1, n_z)
+    ]
+    z_far = lax.rem(z + PAIR, n_z)
+    z_near = z + 1 - 2 * lax.rem(z, PAIR)
+    near = (z_near * PAIR + y, t)
+    residual_a = send(residual_ref, res_all.at[x, c, z], z_id(PAIR))
+
+    latent_core = []
+    for step in range(1, n_z):
+        for copy in latent_z[step - 1]:
+            copy.wait_recv()
+        owner = lax.rem(z + n_z - step, n_z) * PAIR + y
+        latent_y.append(pass_latent(owner, beside))
+        latent_core.extend(pass_latent(owner, sibling))
     weight_y = [
         send(gate_ref.at[:, my_piece], gate_all.at[mine], beside),
         send(up_ref.at[:, my_piece], up_all.at[mine], beside),
-        send(down_ref.at[my_piece], down_all.at[:, mine], beside),
+        send(down_ref.at[my_piece], down_all.at[0, :, down_cols], beside),
     ]
-
-    latent_core = []
-    for step in range(1, n_sp):
-        for copy in latent_copies[step - 1]:
+    for step in range(n_z):
+        for copy in latent_y[step]:
             copy.wait_recv()
-        place = token_half(lax.rem(s + n_sp - step, n_sp))
-        latent_core.append(send(lat_all.at[place], lat_all.at[place], sibling))
-        latent_core.append(send(rot_all.at[place], rot_all.at[place], sibling))
+        owner = lax.rem(z + n_z - step, n_z) * PAIR + 1 - y
+        latent_core.extend(pass_latent(owner, sibling))
     weight_core = send(output_weight_ref, out_all.at[x, c], sibling)
     for copy in locals_first:
         copy.wait()
@@ -337,7 +362,6 @@
     rot_keys = (
         rot_raw.astype(f32) * cos_ref[:, :rot_width] + rot_swapped * sin_ref[:, :rot_width]
     ).astype(jnp.bfloat16)
-    here = pl.ds(pl.multiple_of(s * rows, rows), rows)
     turn_raw = turn_ref[...]
     turn_swapped = jnp.dot(turn_raw, swap, preferred_element_type=f32)
     turned = (turn_raw.astype(f32) * cos_ref[here, :] + turn_swapped * sin_ref[here, :]).astype(
@@ -377,43 +401,41 @@
 
     mix_z = [send(mix_all.at[x, c, z], mix_all.at[x, c, z], z_id(k)) for k in range(1, n_z)]
 
-    def piece_of(step):
-        return pl.ds(first(lax.rem(z + step, n_z)), width)
-
-    gate_z = [
-        send(gate_ref.at[:, piece_of(k)], gate_all.at[mine], z_id(k)) for k in range(1, n_z)
+    def relay(copies, buffer, step):
+        copies[step - 1].wait_recv()
+        block = buffer.at[span(lax.rem(z + n_z - step, n_z) * PAIR + y)]
+        return send(block, block, beside)
+
+    gate_y = [relay(gate_z, gate_all, k) for k in range(1, n_z)]
+    residual_a.wait_recv()
+    locals_rest[0].wait()
+    residual_b = [
+        send(res_all.at[x, c, block], res_all.at[x, c, block], near) for block in (z, z_far)
     ]
     up_z = [send(up_ref.at[:, piece_of(k)], up_all.at[mine], z_id(k)) for k in range(1, n_z)]
     down_z = [
-        send(down_ref.at[piece_of(k)], down_all.at[:, mine], z_id(k)) for k in range(1, n_z)
+        send(down_ref.at[piece_of(k)], down_all.at[k, :, down_cols], z_id(k))
+        for k in range(1, n_z)
     ]
 
-    for copy in residual_z:
-        copy.wait_recv()
-    for copy in locals_rest:
+    for copy in locals_rest[1:]:
         copy.wait()
-    residual_x = send(res_all.at[x, c], res_all.at[x, c], across)
+    weight_x.wait_recv()
+    weight_far = send(out_all.at[1 - x, c], out_all.at[1 - x, c], sibling)
     for copy in mix_z:
         copy.wait_recv()
     mix_x = send(mix_all.at[x, c], mix_all.at[x, c], across)
     mix_core = send(mix_all.at[x, c], mix_all.at[x, c], sibling)
+    for copy in residual_b:
+        copy.wait_recv()
+    residual_x = send(res_all.at[x, c], res_all.at[x, c], across)
     residual_core = send(res_all.at[x, c], res_all.at[x, c], sibling)
-    weight_x.wait_recv()
-    weight_far = send(out_all.at[1 - x, c], out_all.at[1 - x, c], sibling)
     mix_x.wait_recv()
     mix_far = send(mix_all.at[1 - x, c], mix_all.at[1 - x, c], sibling)
+    up_y = [relay(up_z, up_all, 1)]
     residual_x.wait_recv()
     residual_far = send(res_all.at[1 - x, c], res_all.at[1 - x, c], sibling)
-
-    def relay(copies, buffer, columns):
-        passed = []
-        for step in range(1, n_z):
-            copies[step - 1].wait_recv()
-            place = span(lax.rem(z + n_z - step, n_z) * PAIR + y)
-            block = buffer.at[:, place] if columns else buffer.at[place]
-            passed.append(send(block, block, beside))
-        return passed
-
+    up_y += [relay(up_z, up_all, k) for k in range(2, n_z)]
     for copy in (weight_core, weight_far, mix_core, mix_far, residual_core, residual_far):
         copy.wait_recv()
 
@@ -438,9 +460,12 @@
 
     lax.fori_loop(0, n_z, finish_rows, 0)
 
-    gate_y = relay(gate_z, gate_all, False)
-    up_y = relay(up_z, up_all, False)
-    down_y = relay(down_z, down_all, True)
+    def relay_down(step):
+        down_z[step - 1].wait_recv()
+        block = down_all.at[step, :, down_cols]
+        return send(block, block, beside)
+
+    down_y = [weight_y[2], relay_down(1)]
     for copy in gate_y + up_y + weight_y[:2]:
         copy.wait_recv()
 
@@ -457,41 +482,50 @@
         return 0
 
     lax.fori_loop(0, n_z, units, 0)
-    for copy in down_y + weight_y[2:]:
-        copy.wait_recv()
-
+
+    core_copies, x_copies, z_copies = [], [], []
+    for step in range(n_z + 2):
+        n = step - 2
+        if 0 <= n < n_z:
+            x_copies[n].wait_recv()
+            to_z[n] = (to_x[n, :, x].astype(f32) + from_x[n].astype(f32)).astype(jnp.bfloat16)
+            z_copies.append(
+                [
+                    send(to_z.at[n, lax.rem(z + k, n_z)], from_z.at[n, k - 1], z_id(k))
+                    for k in range(1, n_z)
+                ]
+            )
+        n = step - 1
+        if 0 <= n < n_z:
+            core_copies[n].wait_recv()
+            to_x[n] = (part[n, :, :, c].astype(f32) + from_core[n].astype(f32)).astype(
+                jnp.bfloat16
+            )
+            x_copies.append(send(to_x.at[n, :, 1 - x], from_x.at[n], across))
+        n = step
+        if n < n_z:
+            if 2 <= n + 1 < n_z:
+                down_y.append(relay_down(n + 1))
+            down_y[n].wait_recv()
+            product = jnp.dot(hidden[...], down_all[n], preferred_element_type=f32)
+            part[n] = product.astype(jnp.bfloat16).reshape(part.shape[1:])
+            core_copies.append(send(part.at[n, :, :, 1 - c], from_core.at[n], sibling))
+    strip = out_ref.shape[0]
     chunk = part.shape[-1]
-    core_copies = []
-    for n in range(CHUNKS):
-        product = jnp.dot(
-            hidden[...], down_all[:, n * chunk : (n + 1) * chunk], preferred_element_type=f32
-        )
-        part[n] = product.astype(jnp.bfloat16).reshape(part.shape[1:])
-        core_copies.append(send(part.at[n, :, :, 1 - c], from_core.at[n], sibling))
-    x_copies = []
-    for n in range(CHUNKS):
-        core_copies[n].wait_recv()
-        to_x[n] = (part[n, :, :, c].astype(f32) + from_core[n].astype(f32)).astype(jnp.bfloat16)
-        x_copies.append(send(to_x.at[n, :, 1 - x], from_x.at[n], across))
-    z_copies = []
-    for n in range(CHUNKS):
-        x_copies[n].wait_recv()
-        to_z[n] = (to_x[n, :, x].astype(f32) + from_x[n].astype(f32)).astype(jnp.bfloat16)
-        z_copies.append(
-            [
-                send(to_z.at[n, lax.rem(z + k, n_z)], from_z.at[n, k - 1], z_id(k))
-                for k in range(1, n_z)
-            ]
-        )
-    strip = out_ref.shape[0]
     own = pl.ds(pl.multiple_of(z * rows + t * strip, strip), strip)
-    for n in range(CHUNKS):
-        total = to_z[n, z].astype(f32)
+
+    def cols_of(back):
+        return pl.ds(pl.multiple_of(lax.rem(z + 2 * n_z - back, n_z) * chunk, chunk), chunk)
+
+    for n in range(n_z):
+        cols = cols_of(n)
+        summed_up[:, cols] = middle[own, cols].astype(f32) + to_z[n, z].astype(f32)
+    for n in range(n_z):
         for k in range(1, n_z):
             z_copies[n][k - 1].wait_recv()
-            total = total + from_z[n, k - 1].astype(f32)
-        cols = slice(n * chunk, (n + 1) * chunk)
-        out_ref[:, cols] = (middle[own, cols].astype(f32) + total).astype(jnp.bfloat16)
+            cols = cols_of(n + k)
+            summed_up[:, cols] = summed_up[:, cols] + from_z[n, k - 1].astype(f32)
+    out_ref[...] = summed_up[...].astype(jnp.bfloat16)
     for copy in sent:
         copy.wait_send()
 
@@ -536,17 +570,18 @@
     tiles = gate_weight.shape[1] // LANES
     width = -(-tiles // n_z) * LANES
     slab = rows * n_z
-    chunk = d_model // CHUNKS
+    chunk = d_model // n_z
     bf16 = jnp.bfloat16
-    n_copies = 2 * 2 * (n_sp - 1) + 8 * (n_z - 1) + 16 + CHUNKS * (n_z + 1)
+    n_copies = 4 * n_sp + 8 * n_z + 20 + n_z * (n_z + 1)
     vmem = pl.BlockSpec(memory_space=pltpu.VMEM)
     anywhere = pl.BlockSpec(memory_space=pl.ANY)
     return pl.pallas_call(
         functools.partial(kernel, n_sp),
         out_shape=jax.ShapeDtypeStruct((strip, d_model), bf16),
-        in_specs=[vmem] * 12 + [anywhere] * 5,
+        in_specs=[vmem] * 10 + [anywhere] * 7,
         out_specs=vmem,
         scratch_shapes=[
+            pltpu.VMEM((rows, turn_width), bf16),
             pltpu.VMEM((tokens, latent_width), bf16),
             pltpu.VMEM((tokens, ROT_DIM), bf16),
             pltpu.VMEM((tokens, content), bf16),
@@ -558,14 +593,15 @@
             pltpu.VMEM((slab, d_model), bf16),
             pltpu.VMEM((d_model, width), bf16),
             pltpu.VMEM((d_model, width), bf16),
-            pltpu.VMEM((width, d_model), bf16),
+            pltpu.VMEM((n_z, width, chunk), bf16),
             pltpu.VMEM((slab, width), bf16),
-            pltpu.VMEM((CHUNKS, n_z, PAIR, PAIR, strip, chunk), bf16),
-            pltpu.VMEM((CHUNKS, n_z, PAIR, strip, chunk), bf16),
-            pltpu.VMEM((CHUNKS, n_z, PAIR, strip, chunk), bf16),
-            pltpu.VMEM((CHUNKS, n_z, strip, chunk), bf16),
-            pltpu.VMEM((CHUNKS, n_z, strip, chunk), bf16),
-            pltpu.VMEM((CHUNKS, n_z - 1, strip, chunk), bf16),
+            pltpu.VMEM((n_z, n_z, PAIR, PAIR, strip, chunk), bf16),
+            pltpu.VMEM((n_z, n_z, PAIR, strip, chunk), bf16),
+            pltpu.VMEM((n_z, n_z, PAIR, strip, chunk), bf16),
+            pltpu.VMEM((n_z, n_z, strip, chunk), bf16),
+            pltpu.VMEM((n_z, n_z, strip, chunk), bf16),
+            pltpu.VMEM((n_z, n_z - 1, strip, chunk), bf16),
+            pltpu.VMEM((strip, d_model), jnp.float32),
             pltpu.SemaphoreType.DMA((n_copies,)),
             pltpu.SemaphoreType.DMA((n_copies,)),
             pltpu.SemaphoreType.DMA((8,)),
@@ -576,9 +612,7 @@
         name="layer",
     )(
         query_content,
-        query_rotary,
         key_latent,
-        rotary_key,
         latent_gain.reshape(1, -1),
         key_weight,
         value_weight,
@@ -592,6 +626,8 @@
         gate_weight,
         up_weight,
         down_weight,
+        query_rotary,
+        rotary_key,
     )
 
 
@@ -602,10 +638,10 @@
         residual, gate_weight = arrays[0], arrays[11]
         fits = (
             n_tp == PAIR * PAIR
-            and n_sp % PAIR == 0
+            and n_sp == PAIR**3
+            and gate_weight.shape[0] * n_sp == residual.shape[1]
             and gate_weight.shape[0] % LANES == 0
             and gate_weight.shape[1] % LANES == 0
-            and residual.shape[1] % (CHUNKS * LANES) == 0
         )
         if fits:
             return fused(n_sp, *arrays)

time: 134 us -> 112 us (0.84)
  Pallas kernels: 130 us -> 108 us
    pallas_call x1, Pallas kernels: 130 us -> 108 us  [fused(): pl.pallas_call(functools.partial(kernel, n_sp), out_shape=jax.ShapeDtypeS...]
where the time goes in v2:
time: 112 us
  Pallas kernels  108 us (96%)
  local copies, waits for them, and re-layouts  3.75 us (3%)
    pallas_call x1, Pallas kernels, fused(): pl.pallas_call(functools.partial(kernel, n_sp), out_shape=jax.ShapeDtypeS...  108 us
    unnamed x5, local copies, waits for them, and re-layouts  3.75 us

profile of v2, /device:TPU:0, one launch (start us, length us, event | category | flops | bytes accessed | tf_op | source)
XLA Modules:
  0.0 111.8 jit_solution(3891759829944476987)
XLA Ops:
  0.0 0.0 copy-start
  0.0 1.5 %copy.18.turn_hbm = bf16[128,96]{1,0:T(8,128)(2,1)} copy(bf16[128,96]{0,1:T(8,128)(2,1)} %param.19) | data formatting | bytes 49152 | tf_op args[2]
  1.5 0.0 copy-done
  1.5 0.7 copy.19.rotary_ref
  2.2 108.0 %layer.1 = bf16[32,2048]{1,0:T(8,128)(2,1)} custom-call(bf16[128,256]{1,0:T(8,128)(2,1)} %query_ref.1, bf16[128,512]{1,0:T(8,128)(2,1)} %latent_ref.1, f32[1,512]{1,0:T(1,128)} %bitcast.4, bf16[512,256]{1,0:T(8,128)(2,1)} %key_weight_ref.1, bf16[512,256]{1,0:T(8,128)(2,1)} %value_weight_ref.1, f32[1,256]{1,0:T(1,128)} %bitcast.5, f32[1,2048]{1,0:T(1,128)} %bitcast.3, ...), custom_call_target="tpu_custom_call" | custom-call | tf_op jit(solution)/shard_map/layer/pallas_call | solution.py:578
  110.2 1.6 %copy.21 = bf16[32,2048]{1,0:T(8,128)(2,1)} copy(bf16[32,2048]{1,0:T(8,128)(2,1)} %layer.1) | data formatting | bytes 262144
Async XLA Ops:
  0.0 1.5 %copy-start = (bf16[128,32]{0,1:T(8,128)(2,1)S(1)}, bf16[128,32]{0,1:T(8,128)(2,1)}, u32[]{:S(2)}) copy-start(bf16[128,32]{0,1:T(8,128)(2,1)} %param.21) | copy-start | bytes 24580

commit v3 on v2

--- a/solution.py
+++ b/solution.py
@@ -308,13 +308,13 @@
     latent_z = [send_latent(z_id(k)) for k in range(1, n_z)]
     latent_y = [send_latent(beside)]
     weight_x = send(output_weight_ref, out_all.at[x, c], across)
-    gate_z = [
-        send(gate_ref.at[:, piece_of(k)], gate_all.at[mine], z_id(k)) for k in range(1, n_z)
-    ]
     z_far = lax.rem(z + PAIR, n_z)
     z_near = z + 1 - 2 * lax.rem(z, PAIR)
     near = (z_near * PAIR + y, t)
     residual_a = send(residual_ref, res_all.at[x, c, z], z_id(PAIR))
+    gate_z = [
+        send(gate_ref.at[:, piece_of(k)], gate_all.at[mine], z_id(k)) for k in range(1, n_z)
+    ]
 
     latent_core = []
     for step in range(1, n_z):
@@ -328,6 +328,11 @@
         send(up_ref.at[:, my_piece], up_all.at[mine], beside),
         send(down_ref.at[my_piece], down_all.at[0, :, down_cols], beside),
     ]
+    residual_a.wait_recv()
+    locals_rest[0].wait()
+    residual_b = [
+        send(res_all.at[x, c, block], res_all.at[x, c, block], near) for block in (z, z_far)
+    ]
     for step in range(n_z):
         for copy in latent_y[step]:
             copy.wait_recv()
@@ -401,23 +406,18 @@
 
     mix_z = [send(mix_all.at[x, c, z], mix_all.at[x, c, z], z_id(k)) for k in range(1, n_z)]
 
-    def relay(copies, buffer, step):
-        copies[step - 1].wait_recv()
-        block = buffer.at[span(lax.rem(z + n_z - step, n_z) * PAIR + y)]
-        return send(block, block, beside)
-
-    gate_y = [relay(gate_z, gate_all, k) for k in range(1, n_z)]
-    residual_a.wait_recv()
-    locals_rest[0].wait()
-    residual_b = [
-        send(res_all.at[x, c, block], res_all.at[x, c, block], near) for block in (z, z_far)
-    ]
     up_z = [send(up_ref.at[:, piece_of(k)], up_all.at[mine], z_id(k)) for k in range(1, n_z)]
     down_z = [
         send(down_ref.at[piece_of(k)], down_all.at[k, :, down_cols], z_id(k))
         for k in range(1, n_z)
     ]
 
+    def relay(copies, buffer, step):
+        copies[step - 1].wait_recv()
+        block = buffer.at[span(lax.rem(z + n_z - step, n_z) * PAIR + y)]
+        return send(block, block, beside)
+
+    gate_y = [relay(gate_z, gate_all, k) for k in range(1, n_z)]
     for copy in locals_rest[1:]:
         copy.wait()
     weight_x.wait_recv()

time: 112 us -> 113 us (level)
  no operation moved by 1% of the time
where the time goes in v3:
time: 113 us; the launch traced here: 112 us
  Pallas kernels  109 us (96%)
  local copies, waits for them, and re-layouts  3.75 us (3%)
    pallas_call x1, Pallas kernels, fused(): pl.pallas_call(functools.partial(kernel, n_sp), out_shape=jax.ShapeDtypeS...  109 us
    unnamed x5, local copies, waits for them, and re-layouts  3.75 us

profile of v3, /device:TPU:0, one launch (start us, length us, event | category | flops | bytes accessed | tf_op | source)
XLA Modules:
  0.0 112.4 jit_solution(18360323088584908687)
XLA Ops:
  0.0 0.0 copy-start
  0.0 1.5 %copy.18.turn_hbm = bf16[128,96]{1,0:T(8,128)(2,1)} copy(bf16[128,96]{0,1:T(8,128)(2,1)} %param.19) | data formatting | bytes 49152 | tf_op args[2]
  1.5 0.0 copy-done
  1.5 0.7 copy.19.rotary_ref
  2.2 108.6 %layer.1 = bf16[32,2048]{1,0:T(8,128)(2,1)} custom-call(bf16[128,256]{1,0:T(8,128)(2,1)} %query_ref.1, bf16[128,512]{1,0:T(8,128)(2,1)} %latent_ref.1, f32[1,512]{1,0:T(1,128)} %bitcast.4, bf16[512,256]{1,0:T(8,128)(2,1)} %key_weight_ref.1, bf16[512,256]{1,0:T(8,128)(2,1)} %value_weight_ref.1, f32[1,256]{1,0:T(1,128)} %bitcast.5, f32[1,2048]{1,0:T(1,128)} %bitcast.3, ...), custom_call_target="tpu_custom_call" | custom-call | tf_op jit(solution)/shard_map/layer/pallas_call | solution.py:578
  110.8 1.6 %copy.21 = bf16[32,2048]{1,0:T(8,128)(2,1)} copy(bf16[32,2048]{1,0:T(8,128)(2,1)} %layer.1) | data formatting | bytes 262144
Async XLA Ops:
  0.0 1.5 %copy-start = (bf16[128,32]{0,1:T(8,128)(2,1)S(1)}, bf16[128,32]{0,1:T(8,128)(2,1)}, u32[]{:S(2)}) copy-start(bf16[128,32]{0,1:T(8,128)(2,1)} %param.21) | copy-start | bytes 24580
